TPU v7x, 32 devices: a whole 2x2x4 slice. The times are simulated.
32 devices in a mesh: ep: 8 (over z, x), tp: 4 (over y, core).
Axes of the slice: x: 2, y: 2, z: 4, core: 2. Of those that a mesh axis runs over, the one named last changes fastest.
Arguments:
- tokens: bfloat16 [128, 2048], P('ep'), may hold values from -6 to 6
- attn_gain: float32 [2048], replicated, may hold values from 0.1 to 1.9
- w_query: bfloat16 [2048, 1024], P(None, 'tp'), may hold values from -0.125 to 0.125
- stick_bias: float32 [16], P('tp'), may hold values from -8.5 to -2.5
- kv_cache: bfloat16 [128, 8, 1024, 128], P('ep', 'tp'), may hold values from -6 to 6
- lengths: int32 [128], P('ep'), may hold values from 1 to 1024, as said below
- head_gain: float32 [1024], P('tp'), may hold values from 0.1 to 1.9
- w_attn_out: bfloat16 [1024, 2048], P('tp'), may hold values from -0.1875 to 0.1875
- ffn_gain: float32 [2048], replicated, may hold values from 0.1 to 1.9
- route_expert: int32 [128, 2], P('ep'), may hold values from 0 to 31, as said below
- route_weight: bfloat16 [128, 2], P('ep'), may hold values from 0.049804688 to 1
- w_exp_gate: bfloat16 [32, 2048, 2048], P('ep', None, 'tp'), may hold values from -0.125 to 0.125
- w_exp_up: bfloat16 [32, 2048, 2048], P('ep', None, 'tp'), may hold values from -0.125 to 0.125
- w_exp_down: bfloat16 [32, 2048, 2048], P('ep', 'tp'), may hold values from -0.125 to 0.125
- branch_gate: bfloat16 [2048], replicated, may hold values from -0.125 to 0.125
- w_dense_gate: bfloat16 [8192, 2048], P(('ep', 'tp')), may hold values from -0.125 to 0.125
- w_dense_up: bfloat16 [8192, 2048], P(('ep', 'tp')), may hold values from -0.125 to 0.125
- w_dense_down: bfloat16 [8192, 2048], P(('ep', 'tp')), may hold values from -0.125 to 0.125
Outputs:
- mixed: bfloat16 [128, 2048], P('ep', 'tp')
Inputs may be any that keep to these rules, and one draw needn't show every extreme that they name: `route_expert`: each row names 2 different experts of one group (expert x lies in group x // 8). The rows of one index of ep name no expert more than 2 times; one group, the same for every index of ep, has each of its experts named exactly 2 times by the rows of every index of ep. `lengths`: some sequence has length 1024.
All inputs are finite; a program needn't handle non-finite values.
Results may differ from a plain program's by a relative error of at most 0.0076.
Values may be sent and summed in bfloat16 or wider, within the bound.
A program may use at most 128 MiB of HBM per device.

v0:
```python
import math

import jax
import jax.numpy as jnp
from jax import lax
from jax.sharding import PartitionSpec as P

HEADS = 16
HEAD = 64
KV_HEADS = 8
CAP = 2


epsilon = 1e-06
highest = lax.Precision.HIGHEST


def rms_scale(matrix, gain):
    wide = matrix.astype(jnp.float32)
    return wide * lax.rsqrt(jnp.mean(wide * wide, axis=-1, keepdims=True) + epsilon) * gain


def stick_attend(query_rows, key_cols, value_cols, bias_grid, lengths):
    scores = jnp.einsum("shge,shke->shgk", query_rows, key_cols, preferred_element_type=jnp.float32)
    scores = scores / math.sqrt(HEAD) + bias_grid[None, :, :, None]
    position = lax.broadcasted_iota(jnp.int32, scores.shape, 3)
    valid_keys = position < lengths[:, None, None, None]
    log_keep = jnp.where(valid_keys, -jax.nn.softplus(scores), 0.0)
    later_sum = lax.cumsum(log_keep, axis=3, reverse=True) - log_keep
    weights = jnp.where(valid_keys, jnp.exp(jax.nn.log_sigmoid(scores) + later_sum), 0.0).astype(
        jnp.bfloat16
    )
    return jnp.einsum("shgk,shke->shge", weights, value_cols, preferred_element_type=jnp.float32)


def slot_table(routes, expert_ids, capacity):
    id_count = expert_ids.shape[0]
    hit_table = (routes[..., None] == expert_ids).astype(jnp.int32)
    per_row = jnp.sum(hit_table, axis=-2)
    earlier = jnp.cumsum(per_row, axis=-2) - per_row
    slot_rank = jnp.sum(hit_table * earlier[..., None, :], axis=-1)
    local_index = jnp.sum(hit_table * jnp.arange(id_count, dtype=jnp.int32), axis=-1)
    found_any = jnp.sum(hit_table, axis=-1)
    slot_index = jnp.where(found_any > 0, local_index * capacity + slot_rank, -1)
    return (slot_index[..., None] == jnp.arange(id_count * capacity, dtype=jnp.int32)).astype(
        jnp.float32
    )


def expert_apply(expert_rows, w_exp_gate, w_exp_up, w_exp_down):
    gate_pre = jnp.einsum(
        "bxcd,xdf->bxcf", expert_rows, w_exp_gate, preferred_element_type=jnp.float32
    )
    up_pre = jnp.einsum("bxcd,xdf->bxcf", expert_rows, w_exp_up, preferred_element_type=jnp.float32)
    hidden = (jax.nn.silu(gate_pre) * up_pre).astype(jnp.bfloat16)
    return jnp.einsum("bxcf,xfd->bxcd", hidden, w_exp_down, preferred_element_type=jnp.float32)


def dense_hidden(matrix, w_gate_rows, w_up_rows):
    contract = (((1,), (1,)), ((), ()))
    gate_pre = lax.dot_general(matrix, w_gate_rows, contract, preferred_element_type=jnp.float32)
    up_pre = lax.dot_general(matrix, w_up_rows, contract, preferred_element_type=jnp.float32)
    return (jax.nn.silu(gate_pre) * up_pre).astype(jnp.bfloat16)


def gather_all(normed2, route_expert, route_weight, branch):
    return (
        lax.all_gather(normed2, "ep", axis=0, tiled=True),
        lax.all_gather(route_expert, "ep", axis=0, tiled=True),
        lax.all_gather(route_weight, "ep", axis=0, tiled=True),
        lax.all_gather(branch, "ep", axis=0, tiled=True),
    )


def joint_sum(term_rows):
    return lax.psum_scatter(term_rows, ("ep", "tp"), scatter_dimension=0, tiled=True)


def dense_term(all_rows, all_branch, w_dense_gate, w_dense_up, w_dense_down, ep_count, tp_count):
    seq_rows = all_rows.shape[0] // ep_count
    hidden = dense_hidden(all_rows, w_dense_gate, w_dense_up)
    local_units = hidden.shape[1]
    down_cols = w_dense_down.reshape(local_units, tp_count, -1)
    term_sum = jnp.einsum(
        "bsf,fnd->bnsd",
        hidden.reshape(ep_count, seq_rows, local_units),
        down_cols,
        preferred_element_type=jnp.float32,
    )
    return term_sum * all_branch.astype(jnp.float32).reshape(ep_count, 1, seq_rows, 1)


def expert_term(
    all_rows, all_routes, all_weights, w_exp_gate, w_exp_up, w_exp_down, ep_count, tp_count
):
    seq_rows = all_rows.shape[0] // ep_count
    experts_here = w_exp_gate.shape[0]
    own_ids = lax.axis_index("ep") * experts_here + jnp.arange(experts_here, dtype=jnp.int32)
    table = slot_table(all_routes.reshape(ep_count, seq_rows, -1), own_ids, CAP)
    row_blocks = all_rows.reshape(ep_count, seq_rows, -1)
    model_width = row_blocks.shape[2]
    buffer = jnp.einsum(
        "bskc,bsd->bcd", table.astype(jnp.bfloat16), row_blocks, preferred_element_type=jnp.float32
    ).astype(jnp.bfloat16)
    partial_value = expert_apply(
        buffer.reshape(ep_count, experts_here, CAP, model_width), w_exp_gate, w_exp_up, w_exp_down
    )
    partial_value = partial_value.reshape(
        ep_count, experts_here * CAP, tp_count, model_width // tp_count
    )
    combine = jnp.einsum(
        "bskc,bsk->bcs",
        table,
        all_weights.astype(jnp.float32).reshape(ep_count, seq_rows, -1),
        precision=highest,
    )
    return jnp.einsum("bcs,bcnd->bnsd", combine, partial_value, precision=highest)


def shards(
    tokens,
    attn_gain,
    w_query,
    stick_bias,
    kv_cache,
    lengths,
    head_gain,
    w_attn_out,
    ffn_gain,
    route_expert,
    route_weight,
    w_exp_gate,
    w_exp_up,
    w_exp_down,
    branch_gate,
    w_dense_gate,
    w_dense_up,
    w_dense_down,
):
    ep_count = lax.axis_size("ep")
    tp_count = lax.axis_size("tp")
    seq_rows, model_width = tokens.shape
    part_width = model_width // tp_count
    kv_local = kv_cache.shape[1]
    group_size = HEADS // KV_HEADS
    normed = rms_scale(tokens, attn_gain).astype(jnp.bfloat16)
    query_rows = jnp.dot(normed, w_query, preferred_element_type=jnp.float32).astype(jnp.bfloat16)
    query_rows = query_rows.reshape(seq_rows, kv_local, group_size, HEAD)
    head_out = stick_attend(
        query_rows,
        kv_cache[..., :HEAD],
        kv_cache[..., HEAD:],
        stick_bias.reshape(kv_local, group_size),
        lengths,
    )
    head_out = head_out * lax.rsqrt(jnp.mean(head_out * head_out, axis=-1, keepdims=True) + epsilon)
    head_out = head_out * head_gain.reshape(kv_local, group_size, HEAD)
    head_rows = head_out.astype(jnp.bfloat16).reshape(seq_rows, kv_local * group_size * HEAD)
    attention = lax.psum(jnp.dot(head_rows, w_attn_out, preferred_element_type=jnp.float32), "tp")
    residual = tokens.astype(jnp.float32) + attention
    normed2 = rms_scale(residual, ffn_gain).astype(jnp.bfloat16)
    branch = jax.nn.sigmoid(
        jnp.dot(normed2, branch_gate, preferred_element_type=jnp.float32)
    ).astype(jnp.bfloat16)
    residual_cols = lax.dynamic_slice_in_dim(
        residual, lax.axis_index("tp") * part_width, part_width, 1
    )
    all_rows, all_routes, all_weights, all_branch = gather_all(
        normed2, route_expert, route_weight, branch
    )
    term_sum = expert_term(
        all_rows, all_routes, all_weights, w_exp_gate, w_exp_up, w_exp_down, ep_count, tp_count
    )
    term_sum = term_sum + dense_term(
        all_rows, all_branch, w_dense_gate, w_dense_up, w_dense_down, ep_count, tp_count
    )
    mixed = joint_sum(term_sum.reshape(-1, part_width))
    return (residual_cols + mixed).astype(jnp.bfloat16)


def solution(mesh):
    return jax.shard_map(
        shards,
        mesh=mesh,
        in_specs=(
            P("ep", None),
            P(),
            P(None, "tp"),
            P("tp"),
            P("ep", "tp", None, None),
            P("ep"),
            P("tp"),
            P("tp", None),
            P(),
            P("ep", None),
            P("ep", None),
            P("ep", None, "tp"),
            P("ep", None, "tp"),
            P("ep", "tp", None),
            P(),
            P(("ep", "tp"), None),
            P(("ep", "tp"), None),
            P(("ep", "tp"), None),
        ),
        out_specs=P("ep", "tp"),
        check_vma=False,
    )
```

profile of v0, /device:TPU:0, one launch (start us, length us, event | category | flops | bytes accessed | tf_op | source)
XLA Modules:
  0.0 356.7 jit_solution(9556531251418812359)
XLA Ops:
  6.5 1.1 fusion.47
  7.6 0.7 add.93
  8.4 0.8 mul.129
  9.1 1.6 convolution_convert_fusion.1
  10.8 5.7 %fusion.43 = (f32[16,2,2,1024]{3,2,1,0:T(2,128)S(1)}, f32[16,2,2,1024]{3,2,1,0:T(2,128)S(1)}) fusion(s32[16]{0:T(128)} %param.23, f32[2,2]{1,0:T(2,128)S(1)} %add.93, bf16[16,2,2,64]{3,2,1,0:T(2,128)(2,1)S(1)} %reshape.92, bf16[16,2,1024,128]{3,2,1,0:T(8,128)(2,1)} %param.22), kind=kOutput, calls=%fused_computation.41 | convolution fusion | flops 9109504 | bytes 8921168 | tf_op jit(solution)/shard_map/shge,shke->shgk/dot_general | solution.py:24
  16.5 0.2 reshape.93
  16.7 79.2 %reduce-window.6 = f32[16,2,2,8,128]{4,3,2,1,0:T(8,128)S(1)} reduce-window(f32[16,2,2,8,128]{4,3,2,1,0:T(8,128)S(1)} %reshape.93, f32[]{:T(128)} %constant.17.clone.1), window={size=1x1x1x1x128 pad=0_0x0_0x0_0x0_0x0_127}, to_apply=%region_1.2 | reduce-window | flops 8323072 | bytes 524292 | tf_op jit(solution)/shard_map/reduce-window
  95.9 0.3 copy.73
  96.5 0.1 reduce_window_sum.26
  96.7 7.3 %multiply_reduce_fusion.1 = (f32[16,2,2]{2,1,0:T(2,128)S(1)}, f32[16,2,2,64]{3,2,1,0:T(2,128)S(1)}) fusion(bf16[16,2,1024,128]{3,2,1,0:T(8,128)(2,1)} %param.22, f32[16,2,2,1024]{3,2,1,0:T(2,128)S(1)} %reduce_window_sum.26, f32[16,2,2,1024]{3,2,1,0:T(2,128)S(1)} %get-tuple-element.13, s32[16]{0:T(128)S(1)} %copy-done.8), kind=kOutput, calls=%fused_computation.71 | convolution fusion | flops 9772992 | bytes 8929600 | tf_op jit(solution)/shard_map/shgk,shke->shge/dot_general | solution.py:33
  104.4 0.9 fusion.61
  105.4 22.3 %all-gather.1 = bf16[8,16,2]{1,2,0:T(2,128)(2,1)S(1)} all-gather(bf16[1,16,2]{1,2,0:T(2,128)(2,1)S(1)} %bitcast.108), channel_id=1, replica_groups=mesh['ep'=8,'tp'=4] {'ep'}, dimensions={0}, use_global_device_ids=true | all-gather | bytes 576 | tf_op jit(solution)/shard_map/all_gather | solution.py:70
  127.7 16.3 %all-gather = s32[8,16,2]{1,2,0:T(2,128)S(1)} all-gather(s32[1,16,2]{1,2,0:T(2,128)S(1)} %bitcast.107), channel_id=1, replica_groups=mesh['ep'=8,'tp'=4] {'ep'}, dimensions={0}, use_global_device_ids=true | all-gather | bytes 1152 | tf_op jit(solution)/shard_map/all_gather | solution.py:69
  144.1 0.1 copy.79
  144.2 0.7 reduce-window_subtract_fusion
  145.1 0.6 dynamic-slice
  146.5 1.0 multiply_reduce_fusion
  147.6 31.3 %all_gather.13 = bf16[128,2048]{1,0:T(8,128)(2,1)S(1)} all-gather(bf16[16,2048]{1,0:T(8,128)(2,1)S(1)} %multiply_convert_fusion), channel_id=1, replica_groups=mesh['ep'=8,'tp'=4] {'ep'}, dimensions={0}, use_global_device_ids=true | all-gather | bytes 589824 | tf_op jit(solution)/shard_map/all_gather | solution.py:68
  178.9 0.1 fusion.35
  179.0 0.2 dynamic-update-slice
  179.3 19.4 %all-reduce = bf16[128]{0:T(256)(128)(2,1)S(1)} all-reduce(bf16[128]{0:T(256)(128)(2,1)S(1)} %dynamic-update-slice), channel_id=1, replica_groups=mesh['ep'=8,'tp'=4] {'ep'}, use_global_device_ids=true, to_apply=%add | all-reduce | flops 128 | bytes 512
  198.8 0.5 fusion.62
  199.3 0.2 fusion.63
  199.5 0.2 copy.97
  199.6 1.7 fusion.24
  201.4 4.7 %fusion.12 = f32[8,4,2,512]{3,0,2,1:T(8,128)S(1)} fusion(bf16[8,4,2,2048]{3,0,2,1:T(8,128)(2,1)S(1)} %bitcast.100, bf16[4,2048,512]{2,1,0:T(8,128)(2,1)} %param.29), kind=kOutput, calls=%fused_computation.15 | convolution fusion | flops 134217728 | bytes 8781824 | tf_op jit(solution)/shard_map/bxcd,xdf->bxcf/dot_general | solution.py:51
  206.1 4.7 %fusion.21 = bf16[8,4,2,512]{3,0,2,1:T(8,128)(2,1)S(1)} fusion(bf16[8,4,2,2048]{3,0,2,1:T(8,128)(2,1)S(1)} %bitcast.101, bf16[4,2048,512]{2,1,0:T(8,128)(2,1)} %param.30, f32[8,4,2,512]{3,0,2,1:T(8,128)S(1)} %fusion.12), kind=kOutput, calls=%fused_computation.19 | convolution fusion | flops 134414336 | bytes 8847360 | tf_op jit(solution)/shard_map/bxcd,xdf->bxcf/dot_general | solution.py:54
  210.8 1.2 fusion
  212.0 1.3 convolution_bitcast_fusion
  213.4 1.3 fusion.11
  214.7 133.8 %reduce-scatter.2.cloned.1.call-done = f32[16,512]{1,0:T(8,128)} async-done(((f32[512,512]{1,0:T(8,128)}), f32[16,512]{1,0:T(8,128)}) %reduce-scatter.2.cloned.1.call-update) | async-done | bytes 32784 | tf_op jit(solution)/shard_map/reduce_scatter | solution.py:76
  348.5 1.4 add_convert_fusion
  (55 shorter events, 1.4 us)
Async XLA Ops:
  6.5 97.9 %copy-start = (bf16[256,2048]{1,0:T(8,128)(2,1)S(1)}, bf16[256,2048]{1,0:T(8,128)(2,1)}, u32[]{:S(2)}) copy-start(bf16[256,2048]{1,0:T(8,128)(2,1)} %param.25) | copy-start | bytes 3145732
  6.5 90.1 %copy-start.8 = (s32[16]{0:T(128)S(1)}, s32[16]{0:T(128)}, u32[]{:S(2)}) copy-start(s32[16]{0:T(128)} %param.23) | copy-start | bytes 196
  6.5 139.9 %all-reduce.3.cloned.1.call-start = ((), (), s32[]{:S(2)}) async-start(), calls=%async_computation.1 | async-start | bytes 262144 | tf_op jit(solution)/shard_map/psum | solution.py:159
  96.6 8.8 %copy-start.7 = (bf16[16,2]{0,1:T(2,128)(2,1)S(1)}, bf16[16,2]{0,1:T(2,128)(2,1)}, u32[]{:S(2)}) copy-start(bf16[16,2]{0,1:T(2,128)(2,1)} %param.28) | copy-start | bytes 196
  96.6 31.0 %copy-start.6 = (s32[16,2]{0,1:T(2,128)S(1)}, s32[16,2]{0,1:T(2,128)}, u32[]{:S(2)}) copy-start(s32[16,2]{0,1:T(2,128)} %param.27) | copy-start | bytes 388
  96.7 47.3 %copy-start.5 = (bf16[2048]{0:T(1024)(128)(2,1)S(1)}, bf16[2048]{0:T(1024)(128)(2,1)}, u32[]{:S(2)}) copy-start(bf16[2048]{0:T(1024)(128)(2,1)} %param.32) | copy-start | bytes 12292
  96.7 48.5 %copy-start.9 = (u32[32]{0:T(128)S(1)}, u32[32]{0:T(128)}, u32[]{:S(2)}) copy-start(u32[32]{0:T(128)} %constant.60) | copy-start | bytes 388
  96.7 49.8 %copy-start.3 = (bf16[16,2048]{1,0:T(8,128)(2,1)S(1)}, bf16[16,2048]{1,0:T(8,128)(2,1)}, u32[]{:S(2)}) copy-start(bf16[16,2048]{1,0:T(8,128)(2,1)} %param.18) | copy-start | bytes 196612
  96.7 50.8 %copy-start.4 = (f32[2048]{0:T(1024)S(1)}, f32[2048]{0:T(1024)}, u32[]{:S(2)}) copy-start(f32[2048]{0:T(1024)} %param.26) | copy-start | bytes 24580
  96.7 102.1 %copy-start.2 = (bf16[256,2048]{1,0:T(8,128)(2,1)S(1)}, bf16[256,2048]{1,0:T(8,128)(2,1)}, u32[]{:S(2)}) copy-start(bf16[256,2048]{1,0:T(8,128)(2,1)} %param.33) | copy-start | bytes 3145732
  105.3 243.2 %reduce-scatter.2.cloned.1.call-start = ((), (), s32[]{:S(2)}) async-start(), calls=%async_computation.2 | async-start | bytes 1081344 | tf_op jit(solution)/shard_map/reduce_scatter | solution.py:76
  201.4 9.5 %slice-start = ((s8[8388608]{0:T(1024)(128)(4,1)}), s8[4194304]{0:T(1024)(128)(4,1)S(1)}, s32[]{:S(2)}) async-start(s8[8388608]{0:T(1024)(128)(4,1)} %bitcast.96), calls=%async_computation.3 | async-start | bytes 8388608
  206.1 4.7 %slice-start.1 = ((s8[8388608]{0:T(1024)(128)(4,1)}), s8[4194304]{0:T(1024)(128)(4,1)S(1)}, s32[]{:S(2)}) async-start(s8[8388608]{0:T(1024)(128)(4,1)} %bitcast.96), calls=%async_computation.4 | async-start | bytes 8388608
  206.1 7.3 %copy-start.1 = (bf16[256,2048]{1,0:T(8,128)(2,1)S(1)}, bf16[256,2048]{1,0:T(8,128)(2,1)}, u32[]{:S(2)}) copy-start(bf16[256,2048]{1,0:T(8,128)(2,1)} %param.35) | copy-start | bytes 3145732
Sparse Core Ops, SparseCore 0:
  105.5 34.4 all-reduce.2
  214.8 133.6 reduce-scatter.1
where the time goes:
time: 357 us
  waiting for transfers between devices  134 us (38%)
  blocking collectives  89.3 us (25%)
  other arithmetic  84 us (24%)
  matrix products  31.2 us (9%)
  between operations  14.4 us (4%)
  local copies, waits for them, and re-layouts  4.01 us (1%)
    reduce_scatter x1, waiting for transfers between devices, joint_sum(): lax.psum_scatter(term_rows, ('ep', 'tp'), scatter_dimension=0, tiled=True)  134 us
    another operation x2, other arithmetic  79.3 us
    all_gather x1, blocking collectives, gather_all(): lax.all_gather(normed2, 'ep', axis=0, tiled=True)  31.3 us
    all_gather x1, blocking collectives, gather_all(): lax.all_gather(route_weight, 'ep', axis=0, tiled=True)  22.3 us
    unnamed x1, blocking collectives  19.4 us
    all_gather x1, blocking collectives, gather_all(): lax.all_gather(route_expert, 'ep', axis=0, tiled=True)  16.3 us
    dot_general x1, matrix products, stick_attend(): jnp.einsum('shgk,shke->shge', weights, value_cols, preferred_element_type...  7.27 us
  transfers between devices with their start and end apart: 2, of which 1 were waited for; matrix products, arithmetic and copies ran while one was open for 0% of the time, Pallas kernels for 0%

commit v1 on v0

v1 whole, which is shorter than its diff:
```python
import functools
import math

import jax
import jax.numpy as jnp
from jax import lax
from jax.experimental import pallas as pl
from jax.experimental.pallas import tpu as pltpu
from jax.sharding import PartitionSpec as P

HEADS = 16
HEAD = 64
KV_HEADS = 8

epsilon = 1e-06
MESH = pl.DeviceIdType.MESH
single = jnp.float32
half = jnp.bfloat16


def softplus(z):
    return jnp.maximum(z, 0.0) + jnp.log1p(jnp.exp(-jnp.abs(z)))


def mul(a, b):
    return jnp.dot(a, b, preferred_element_type=single)


def mul_rows(a, b):
    return lax.dot_general(a, b, (((1,), (1,)), ((), ())), preferred_element_type=single)


def gated(gate_pre, up_pre):
    return (gate_pre / (1.0 + jnp.exp(-gate_pre)) * up_pre).astype(half)


def remote(src, dst, send, recv, axis, peer):
    return pltpu.make_async_remote_copy(
        src_ref=src,
        dst_ref=dst,
        send_sem=send,
        recv_sem=recv,
        device_id={axis: peer},
        device_id_type=MESH,
    )


def layer_kernel(
    ep_n,
    tp_n,
    tokens,
    attn_gain,
    w_query,
    stick_bias,
    kv_cache,
    lengths,
    head_gain,
    w_attn_out,
    ffn_gain,
    route_expert,
    route_weight,
    w_exp_gate,
    w_exp_up,
    w_exp_down,
    branch_gate,
    w_dense_gate,
    w_dense_up,
    w_dense_down,
    out,
    wq,
    kv,
    wo,
    eg,
    eu,
    ed,
    dg,
    du,
    dd,
    grid,
    att,
    att_send,
    att_recv,
    rows_all,
    routes,
    x,
    hidden,
    pair_send,
    pair_recv,
    y_send,
    y_recv,
    own,
    ep_send,
    ep_recv,
    load_sem,
    kv_sem,
    exp_sem,
    att_sems,
    route_sems,
    gather_sems,
    mate_sems,
    far_sems,
    relay_sems,
    pair_sems,
    y_sems,
    ep_sems,
):
    me_ep, me_tp = lax.axis_index("ep"), lax.axis_index("tp")
    mate = me_tp + 1 - 2 * lax.rem(me_tp, 2)
    y_n = tp_n // 2
    seqs, width = tokens.shape
    part = width // tp_n
    rows = ep_n * seqs
    kv_n = kv_cache.shape[1]
    positions = kv_cache.shape[2]
    heads = kv_n * 2
    score_rows = seqs * heads
    experts = w_exp_gate.shape[0]
    tile_seqs = 8 // heads

    def ep_peer(d):
        return lax.rem(me_ep + d, ep_n)

    def tp_peer(d):
        return lax.rem(me_tp + d, tp_n)

    barrier = pltpu.get_barrier_semaphore()
    for d in range(1, ep_n):
        pl.semaphore_signal(barrier, inc=1, device_id={"ep": ep_peer(d)}, device_id_type=MESH)
    for d in range(1, tp_n):
        pl.semaphore_signal(barrier, inc=1, device_id={"tp": tp_peer(d)}, device_id_type=MESH)

    load_q = pltpu.make_async_copy(w_query, wq, load_sem.at[0])
    load_q.start()
    load_kv = []
    for s in range(seqs):
        load_kv.append(pltpu.make_async_copy(kv_cache.at[s], kv.at[s], kv_sem.at[s]))
        load_kv[-1].start()

    wide = tokens[...].astype(single)
    mean_sq = jnp.mean(wide * wide, axis=-1, keepdims=True)
    normed = (wide * lax.rsqrt(mean_sq + epsilon) * attn_gain[...]).astype(half)
    load_q.wait()
    query = mul(normed, wq[...]).astype(half)

    load_o = pltpu.make_async_copy(w_attn_out, wo, load_sem.at[1])
    load_o.start()
    load_d = []
    for i, (src, dst) in enumerate(((w_dense_gate, dg), (w_dense_up, du), (w_dense_down, dd))):
        load_d.append(pltpu.make_async_copy(src, dst, load_sem.at[2 + i]))
        load_d[-1].start()

    exp_pairs = ((w_exp_gate, eg), (w_exp_up, eu), (w_exp_down, ed))

    def exp_load(i, e):
        src, dst = exp_pairs[i]
        return pltpu.make_async_copy(src.at[e], dst.at[e], exp_sem.at[i, e])

    for e in range(experts):
        exp_load(0, e).start()
        exp_load(1, e).start()
    for e in range(experts):
        exp_load(2, e).start()

    spread = lax.broadcasted_iota(jnp.int32, (score_rows, seqs), 0) // heads
    spread = (spread == lax.broadcasted_iota(jnp.int32, (score_rows, seqs), 1)).astype(half)
    fold = lax.broadcasted_iota(jnp.int32, (seqs, score_rows), 1) // heads
    fold = (fold == lax.broadcasted_iota(jnp.int32, (seqs, score_rows), 0)).astype(half)
    row_id = lax.broadcasted_iota(jnp.int32, (score_rows, 128), 0)
    lane_id = lax.broadcasted_iota(jnp.int32, (score_rows, 128), 1)
    head_id = row_id % heads
    odd = head_id % 2 == 1
    query_rep = mul(spread, query)
    blocks = []
    for k in range(kv_n):
        piece = query_rep[:, k * 128 : (k + 1) * 128]
        piece = jnp.where(odd, pltpu.roll(piece, HEAD, 1), piece)
        keep = (lane_id < HEAD) & (head_id // 2 == k)
        blocks.append(jnp.where(keep, piece, 0.0) * (1.0 / math.sqrt(HEAD)))
    query_blk = jnp.concatenate(blocks, axis=1) if kv_n > 1 else blocks[0]

    def cache_of(s):
        return jnp.concatenate([kv[s, k] for k in range(kv_n)], axis=1) if kv_n > 1 else kv[s, 0]

    tile_row = lax.broadcasted_iota(jnp.int32, (8, 128), 0)[:, :1] // heads
    for p in range(score_rows // 8):
        total = None
        q_tile = query_blk[p * 8 : (p + 1) * 8]
        for u in range(tile_seqs):
            s = p * tile_seqs + u
            load_kv[s].wait()
            term = mul_rows(jnp.where(tile_row == u, q_tile, 0.0).astype(half), cache_of(s))
            total = term if total is None else total + term
        grid[p * 8 : (p + 1) * 8, :] = total

    row_col = row_id[:, :1]
    seq_col, head_col = row_col // heads, row_col % heads
    length_col = jnp.zeros_like(row_col)
    for s in range(seqs):
        length_col = jnp.where(seq_col == s, lengths[s], length_col)
    bias_col = jnp.zeros(row_col.shape, single)
    for h in range(heads):
        bias_col = jnp.where(head_col == h, stick_bias[h], bias_col)
    span = 256
    later = lax.broadcasted_iota(jnp.int32, (span, span), 0)
    later = (later >= lax.broadcasted_iota(jnp.int32, (span, span), 1)).astype(half)
    span_lane = lax.broadcasted_iota(jnp.int32, (score_rows, span), 1)
    carry = jnp.zeros(row_col.shape, single)
    for t in reversed(range(positions // span)):
        z = grid[:, t * span : (t + 1) * span] + bias_col
        valid = span_lane + t * span < length_col
        plus = jnp.where(valid, softplus(z), 0.0)
        high = plus.astype(half)
        rest = plus - high.astype(single)
        mid = rest.astype(half)
        low = (rest - mid.astype(single)).astype(half)
        suffix = mul(high, later) + (mul(mid, later) + mul(low, later)) + carry
        carry = suffix[:, :1]
        grid[:, t * span : (t + 1) * span] = jnp.where(valid, jnp.exp(z - suffix), 0.0)

    tiles = []
    for p in range(score_rows // 8):
        total = None
        w_tile = grid[p * 8 : (p + 1) * 8, :]
        for u in range(tile_seqs):
            s = p * tile_seqs + u
            term = mul(jnp.where(tile_row == u, w_tile, 0.0).astype(half), cache_of(s))
            total = term if total is None else total + term
        tiles.append(total)
    head_out = jnp.concatenate(tiles, axis=0)
    blocks = []
    for k in range(kv_n):
        piece = head_out[:, k * 128 : (k + 1) * 128]
        square = jnp.where(lane_id >= HEAD, piece * piece, 0.0)
        scale = lax.rsqrt(jnp.sum(square, axis=-1, keepdims=True) / HEAD + epsilon)
        piece = piece * scale
        piece = jnp.where(odd, piece, pltpu.roll(piece, HEAD, 1))
        piece = piece * head_gain[:, k * 128 : (k + 1) * 128]
        keep = (lane_id // HEAD == head_id % 2) & (head_id // 2 == k)
        blocks.append(jnp.where(keep, piece, 0.0))
    head_rows = jnp.concatenate(blocks, axis=1) if kv_n > 1 else blocks[0]
    head_rows = mul(fold, head_rows.astype(half)).astype(half)
    load_o.wait()
    for c in range(tp_n):
        piece = mul(head_rows, wo[:, c * part : (c + 1) * part])
        att[c] = piece
        att_send[c] = piece.astype(half)

    ids = route_expert[...].astype(single)
    weights = route_weight[...].astype(single)
    lane = lax.broadcasted_iota(jnp.int32, (seqs, 128), 1)
    packed = jnp.where(
        lane == 0,
        ids[:, 0:1],
        jnp.where(
            lane == 1,
            ids[:, 1:2],
            jnp.where(lane == 2, weights[:, 0:1], jnp.where(lane == 3, weights[:, 1:2], 0.0)),
        ),
    )
    routes[me_ep] = packed.astype(half)

    pl.semaphore_wait(barrier, ep_n + tp_n - 2)

    pending = []
    att_copies = []
    for d in range(1, tp_n):
        copy = remote(
            att_send.at[tp_peer(d)],
            att_recv.at[d],
            att_sems.at[0, d],
            att_sems.at[1, d],
            "tp",
            tp_peer(d),
        )
        copy.start()
        att_copies.append(copy)
    route_copies = []
    for d in range(1, ep_n):
        copy = remote(
            routes.at[me_ep],
            routes.at[me_ep],
            route_sems.at[0, d],
            route_sems.at[1, d],
            "ep",
            ep_peer(d),
        )
        copy.start()
        route_copies.append(copy)
    cols = pl.ds(pl.multiple_of(me_tp * part, part), part)
    residual = att[me_tp]
    for d in range(1, tp_n):
        att_copies[d - 1].wait_recv()
        residual = residual + att_recv[d].astype(single)
    residual = tokens[:, cols].astype(single) + residual
    rows_all[me_tp, me_ep] = residual.astype(half)
    pending += att_copies + route_copies

    gather_copies = [None]
    for d in range(1, ep_n):
        copy = remote(
            rows_all.at[me_tp, me_ep],
            rows_all.at[me_tp, me_ep],
            gather_sems.at[0, d],
            gather_sems.at[1, d],
            "ep",
            ep_peer(d),
        )
        copy.start()
        gather_copies.append(copy)
    pending += gather_copies[1:]
    mates, fars, relays = [], {}, []
    for d in range(ep_n):
        source = lax.rem(me_ep + ep_n - d, ep_n)
        if d:
            gather_copies[d].wait_recv()
        block = rows_all.at[me_tp, source]
        for y in range(1, y_n):
            copy = remote(
                block, block, far_sems.at[0, y, d], far_sems.at[1, y, d], "tp", tp_peer(2 * y)
            )
            copy.start()
            fars[y, d] = copy
        copy = remote(block, block, mate_sems.at[0, d], mate_sems.at[1, d], "tp", mate)
        copy.start()
        mates.append(copy)
    for d in range(ep_n):
        source = lax.rem(me_ep + ep_n - d, ep_n)
        for y in range(1, y_n):
            fars[y, d].wait_recv()
            block = rows_all.at[lax.rem(me_tp + tp_n - 2 * y, tp_n), source]
            copy = remote(
                block, block, relay_sems.at[0, y, d], relay_sems.at[1, y, d], "tp", mate
            )
            copy.start()
            relays.append(copy)
    for copy in route_copies + mates + relays:
        copy.wait_recv()
    pending += mates + list(fars.values()) + relays

    square = jnp.zeros((rows, 1), single)
    for c in range(tp_n):
        piece = rows_all[c].reshape(rows, part).astype(single)
        square = square + jnp.sum(piece * piece, axis=-1, keepdims=True)
    scale = lax.rsqrt(square / width + epsilon)
    logit = jnp.zeros((rows, 1), single)
    for c in range(tp_n):
        span_c = slice(c * part, (c + 1) * part)
        piece = rows_all[c].reshape(rows, part).astype(single)
        piece = (piece * scale * ffn_gain[:, span_c]).astype(half)
        x[:, span_c] = piece
        product = piece.astype(single) * branch_gate[:, span_c].astype(single)
        logit = logit + jnp.sum(product, axis=-1, keepdims=True)
    branch = (1.0 / (1.0 + jnp.exp(-logit))).astype(half).astype(single)
    route = routes[...].reshape(rows, 128).astype(single)

    def coefficient(e):
        own_id = (me_ep * experts + e).astype(single)
        first = jnp.where(route[:, 0:1] == own_id, route[:, 2:3], 0.0)
        return first + jnp.where(route[:, 1:2] == own_id, route[:, 3:4], 0.0)

    for load in load_d:
        load.wait()
    dense = gated(mul_rows(x[...], dg[...]), mul_rows(x[...], du[...]))

    def expert_step(e, carried):
        exp_load(0, e).wait()
        exp_load(1, e).wait()
        hidden[e] = gated(mul(x[...], eg[e]), mul(x[...], eu[e]))
        return carried

    lax.fori_loop(0, experts, expert_step, 0)
    for e in range(experts):
        exp_load(2, e).wait()
    coefs = [coefficient(e) for e in range(experts)]

    def chunk(target):
        at = pl.ds(pl.multiple_of(target * part, part), part)
        total = branch * mul(dense, dd[:, at])
        for e in range(experts):
            total = total + coefs[e] * mul(hidden[e], ed[e, :, at])
        return total

    pair_copies = []
    order = list(range(1, y_n)) + [0]
    for y in order:
        pair_send[y] = chunk(lax.rem(mate + 2 * y, tp_n)).astype(half)
        copy = remote(
            pair_send.at[y], pair_recv.at[y], pair_sems.at[0, y], pair_sems.at[1, y], "tp", mate
        )
        copy.start()
        pair_copies.append(copy)
    y_copies = {}
    for copy, y in zip(pair_copies, order):
        total = chunk(tp_peer(2 * y))
        copy.wait_recv()
        total = total + pair_recv[y].astype(single)
        if y == 0:
            own[...] = total.reshape(ep_n, seqs, part)
            continue
        y_send[y] = total.astype(half).reshape(ep_n, seqs, part)
        for d in list(range(1, ep_n)) + [0]:
            copy = remote(
                y_send.at[y, ep_peer(d)],
                y_recv.at[y, ep_peer(d)],
                y_sems.at[0, y, d],
                y_sems.at[1, y, d],
                "tp",
                tp_peer(2 * y),
            )
            copy.start()
            y_copies[y, d] = copy
    pending += pair_copies + list(y_copies.values())
    ep_copies = []
    for d in list(range(1, ep_n)) + [0]:
        target = ep_peer(d)
        total = own[target]
        for y in range(1, y_n):
            y_copies[y, d].wait_recv()
            total = total + y_recv[y, target].astype(single)
        if d == 0:
            residual = residual + total
            continue
        ep_send[d] = total.astype(half)
        copy = remote(
            ep_send.at[d], ep_recv.at[d], ep_sems.at[0, d], ep_sems.at[1, d], "ep", target
        )
        copy.start()
        ep_copies.append(copy)
    for d in range(1, ep_n):
        ep_copies[d - 1].wait_recv()
        residual = residual + ep_recv[d].astype(single)
    out[...] = residual.astype(half)
    for copy in pending + ep_copies:
        copy.wait_send()


def shards(
    tokens,
    attn_gain,
    w_query,
    stick_bias,
    kv_cache,
    lengths,
    head_gain,
    w_attn_out,
    ffn_gain,
    route_expert,
    route_weight,
    w_exp_gate,
    w_exp_up,
    w_exp_down,
    branch_gate,
    w_dense_gate,
    w_dense_up,
    w_dense_down,
):
    ep_n = lax.axis_size("ep")
    tp_n = lax.axis_size("tp")
    seqs, width = tokens.shape
    part = width // tp_n
    rows = ep_n * seqs
    y_n = tp_n // 2
    kv_n, positions = kv_cache.shape[1:3]
    experts = w_exp_gate.shape[0]
    score_rows = seqs * kv_n * (HEADS // KV_HEADS)
    vmem = pl.BlockSpec(memory_space=pltpu.VMEM)
    smem = pl.BlockSpec(memory_space=pltpu.SMEM)
    hbm = pl.BlockSpec(memory_space=pl.ANY)
    dma = pltpu.SemaphoreType.DMA

    def like(array):
        return pltpu.VMEM(array.shape, array.dtype)

    return pl.pallas_call(
        functools.partial(layer_kernel, ep_n, tp_n),
        out_shape=jax.ShapeDtypeStruct((seqs, part), half),
        in_specs=[
            vmem,
            vmem,
            hbm,
            smem,
            hbm,
            smem,
            vmem,
            hbm,
            vmem,
            vmem,
            vmem,
            hbm,
            hbm,
            hbm,
            vmem,
            hbm,
            hbm,
            hbm,
        ],
        out_specs=vmem,
        scratch_shapes=[
            like(w_query),
            like(kv_cache),
            like(w_attn_out),
            like(w_exp_gate),
            like(w_exp_up),
            like(w_exp_down),
            like(w_dense_gate),
            like(w_dense_up),
            like(w_dense_down),
            pltpu.VMEM((score_rows, positions), single),
            pltpu.VMEM((tp_n, seqs, part), single),
            pltpu.VMEM((tp_n, seqs, part), half),
            pltpu.VMEM((tp_n, seqs, part), half),
            pltpu.VMEM((tp_n, ep_n, seqs, part), half),
            pltpu.VMEM((ep_n, seqs, 128), half),
            pltpu.VMEM((rows, width), half),
            pltpu.VMEM((experts, rows, w_exp_gate.shape[2]), half),
            pltpu.VMEM((y_n, rows, part), half),
            pltpu.VMEM((y_n, rows, part), half),
            pltpu.VMEM((y_n, ep_n, seqs, part), half),
            pltpu.VMEM((y_n, ep_n, seqs, part), half),
            pltpu.VMEM((ep_n, seqs, part), single),
            pltpu.VMEM((ep_n, seqs, part), half),
            pltpu.VMEM((ep_n, seqs, part), half),
            dma((5,)),
            dma((seqs,)),
            dma((3, experts)),
            dma((2, tp_n)),
            dma((2, ep_n)),
            dma((2, ep_n)),
            dma((2, ep_n)),
            dma((2, y_n, ep_n)),
            dma((2, y_n, ep_n)),
            dma((2, y_n)),
            dma((2, y_n, ep_n)),
            dma((2, ep_n)),
        ],
        compiler_params=pltpu.CompilerParams(
            collective_id=0, has_side_effects=True, vmem_limit_bytes=60 * 1024 * 1024
        ),
    )(
        tokens,
        attn_gain.reshape(1, -1),
        w_query,
        stick_bias,
        kv_cache,
        lengths,
        head_gain.reshape(1, -1),
        w_attn_out,
        ffn_gain.reshape(1, -1),
        route_expert,
        route_weight,
        w_exp_gate,
        w_exp_up,
        w_exp_down,
        branch_gate.reshape(1, -1),
        w_dense_gate,
        w_dense_up,
        w_dense_down,
    )


def solution(mesh):
    return jax.shard_map(
        shards,
        mesh=mesh,
        in_specs=(
            P("ep", None),
            P(),
            P(None, "tp"),
            P("tp"),
            P("ep", "tp", None, None),
            P("ep"),
            P("tp"),
            P("tp", None),
            P(),
            P("ep", None),
            P("ep", None),
            P("ep", None, "tp"),
            P("ep", None, "tp"),
            P("ep", "tp", None),
            P(),
            P(("ep", "tp"), None),
            P(("ep", "tp"), None),
            P(("ep", "tp"), None),
        ),
        out_specs=P("ep", "tp"),
        check_vma=False,
    )
```

time: 357 us -> 48.2 us (0.14)
  waiting for transfers between devices: 134 us -> 0 us
  blocking collectives: 89.3 us -> 0 us
  other arithmetic: 84 us -> 0 us
  Pallas kernels: 0 us -> 42.6 us
  matrix products: 31.2 us -> 0 us
  between operations: 14.4 us -> 0.01 us
    reduce_scatter x1 -> x0, waiting for transfers between devices: 134 us -> none  [joint_sum(): lax.psum_scatter(term_rows, ('ep', 'tp'), scatter_dimension=0, tiled=True)]
    another operation x4 -> x0, other arithmetic: 80.1 us -> none
    all_gather x3 -> x0, blocking collectives: 69.9 us -> none  [the longest x1 31.3 us: gather_all(): lax.all_gather(normed2, 'ep', axis=0, tiled=True)]
    pallas_call x0 -> x1, Pallas kernels: none -> 42.6 us  [shards(): pl.pallas_call(functools.partial(layer_kernel, ep_n, tp_n), out_shape=jax...]
    dot_general x13 -> x0, matrix products: 31.2 us -> none  [the longest x1 7.27 us: stick_attend(): jnp.einsum('shgk,shke->shge', weights, value_cols, preferred_element_type...]
    unnamed x1 -> x0, blocking collectives: 19.4 us -> none
  transfers between devices with their start and end apart: 2 -> 0, of which waited for: 1 -> 0; matrix products, arithmetic and copies ran while one was open for 0% -> 0% of each run, Pallas kernels for 0% -> 0%
where the time goes in v1:
time: 48.2 us; the launch traced here: 47.9 us
  Pallas kernels  42.6 us (88%)
  local copies, waits for them, and re-layouts  5.28 us (11%)
    pallas_call x1, Pallas kernels, shards(): pl.pallas_call(functools.partial(layer_kernel, ep_n, tp_n), out_shape=jax...  42.6 us
    unnamed x3, local copies, waits for them, and re-layouts  4 us
    reshape x1, local copies, waits for them, and re-layouts, shards(): branch_gate.reshape(1, -1)  1.28 us

profile of v1, /device:TPU:0, one launch (start us, length us, event | category | flops | bytes accessed | tf_op | source)
XLA Modules:
  0.0 47.9 jit_solution(5605103518208114763)
XLA Ops:
  0.0 1.3 %copy.20.route_weight = bf16[16,2]{1,0:T(8,128)(2,1)} copy(bf16[16,2]{0,1:T(2,128)(2,1)} %param.28) | data formatting | bytes 128 | tf_op args[10]
  1.3 1.4 %copy.19.route_expert = s32[16,2]{1,0:T(8,128)} copy(s32[16,2]{0,1:T(2,128)} %param.27) | data formatting | bytes 256 | tf_op args[9]
  2.7 1.3 %reshape.15.branch_gate = bf16[1,2048]{1,0:T(2,128)(2,1)} reshape(bf16[2048]{0:T(1024)(128)(2,1)} %param.32) | data formatting | bytes 8192 | tf_op jit(solution)/shard_map/reshape | solution.py:554
  4.0 42.6 %shard_map.172 = bf16[16,512]{1,0:T(8,128)(2,1)} custom-call(bf16[16,2048]{1,0:T(8,128)(2,1)} %tokens.1, f32[1,2048]{1,0:T(1,128)} %bitcast.3, bf16[2048,256]{1,0:T(8,128)(2,1)} %w_query.1, f32[4]{0:T(128)} %stick_bias.1, bf16[16,2,1024,128]{3,2,1,0:T(8,128)(2,1)} %kv_cache.1, s32[16]{0:T(128)} %lengths.1, f32[1,256]{1,0:T(1,128)} %bitcast.5, ...), custom_call_target="tpu_custom_call" | custom-call | tf_op jit(solution)/shard_map/pallas_call | solution.py:474
  46.6 1.3 %copy.22 = bf16[16,512]{1,0:T(8,128)(2,1)} copy(bf16[16,512]{1,0:T(8,128)(2,1)} %shard_map.172) | data formatting | bytes 32768

commit v2 on v1

--- a/solution.py
+++ b/solution.py
@@ -185,9 +185,11 @@
     for p in range(score_rows // 8):
         total = None
         q_tile = query_blk[p * 8 : (p + 1) * 8]
+        if p * tile_seqs % 4 == 0:
+            for load in load_kv[p * tile_seqs : p * tile_seqs + 4]:
+                load.wait()
         for u in range(tile_seqs):
             s = p * tile_seqs + u
-            load_kv[s].wait()
             term = mul_rows(jnp.where(tile_row == u, q_tile, 0.0).astype(half), cache_of(s))
             total = term if total is None else total + term
         grid[p * 8 : (p + 1) * 8, :] = total
@@ -245,16 +247,22 @@
         att[c] = piece
         att_send[c] = piece.astype(half)
 
-    ids = route_expert[...].astype(single)
-    weights = route_weight[...].astype(single)
+    eye = lax.broadcasted_iota(jnp.int32, (seqs, seqs), 0)
+    eye = eye == lax.broadcasted_iota(jnp.int32, (seqs, seqs), 1)
+
+    def upright(row):
+        return jnp.sum(jnp.where(eye, row.astype(single), 0.0), axis=1, keepdims=True)
+
+    ids = [upright(route_expert[j : j + 1, :]) for j in range(2)]
+    weights = [upright(route_weight[j : j + 1, :]) for j in range(2)]
     lane = lax.broadcasted_iota(jnp.int32, (seqs, 128), 1)
     packed = jnp.where(
         lane == 0,
-        ids[:, 0:1],
+        ids[0],
         jnp.where(
             lane == 1,
-            ids[:, 1:2],
-            jnp.where(lane == 2, weights[:, 0:1], jnp.where(lane == 3, weights[:, 1:2], 0.0)),
+            ids[1],
+            jnp.where(lane == 2, weights[0], jnp.where(lane == 3, weights[1], 0.0)),
         ),
     )
     routes[me_ep] = packed.astype(half)
@@ -343,12 +351,13 @@
         square = square + jnp.sum(piece * piece, axis=-1, keepdims=True)
     scale = lax.rsqrt(square / width + epsilon)
     logit = jnp.zeros((rows, 1), single)
+    branch_row = branch_gate[...].astype(single).reshape(1, width)
     for c in range(tp_n):
         span_c = slice(c * part, (c + 1) * part)
         piece = rows_all[c].reshape(rows, part).astype(single)
         piece = (piece * scale * ffn_gain[:, span_c]).astype(half)
         x[:, span_c] = piece
-        product = piece.astype(single) * branch_gate[:, span_c].astype(single)
+        product = piece.astype(single) * branch_row[:, span_c]
         logit = logit + jnp.sum(product, axis=-1, keepdims=True)
     branch = (1.0 / (1.0 + jnp.exp(-logit))).astype(half).astype(single)
     route = routes[...].reshape(rows, 128).astype(single)
@@ -546,12 +555,12 @@
         head_gain.reshape(1, -1),
         w_attn_out,
         ffn_gain.reshape(1, -1),
-        route_expert,
-        route_weight,
+        route_expert.T,
+        route_weight.T,
         w_exp_gate,
         w_exp_up,
         w_exp_down,
-        branch_gate.reshape(1, -1),
+        branch_gate,
         w_dense_gate,
         w_dense_up,
         w_dense_down,

time: 48.2 us -> 44.2 us (0.917)
  local copies, waits for them, and re-layouts: 5.28 us -> 1.32 us
    unnamed x3 -> x1, local copies, waits for them, and re-layouts: 4 us -> 1.32 us
    reshape x1 -> x0, local copies, waits for them, and re-layouts: 1.28 us -> none  [shards(): branch_gate.reshape(1, -1)]
where the time goes in v2:
time: 44.2 us; the launch traced here: 44 us
  Pallas kernels  42.7 us (97%)
  local copies, waits for them, and re-layouts  1.32 us (3%)
    pallas_call x1, Pallas kernels, shards(): pl.pallas_call(functools.partial(layer_kernel, ep_n, tp_n), out_shape=jax...  42.7 us
    unnamed x1, local copies, waits for them, and re-layouts  1.32 us

profile of v2, /device:TPU:0, one launch (start us, length us, event | category | flops | bytes accessed | tf_op | source)
XLA Modules:
  0.0 44.0 jit_solution(12054766916353427753)
XLA Ops:
  0.0 42.7 %shard_map.172 = bf16[16,512]{1,0:T(8,128)(2,1)} custom-call(bf16[16,2048]{1,0:T(8,128)(2,1)} %tokens.1, f32[1,2048]{1,0:T(1,128)} %bitcast.5, bf16[2048,256]{1,0:T(8,128)(2,1)} %w_query.1, f32[4]{0:T(128)} %stick_bias.1, bf16[16,2,1024,128]{3,2,1,0:T(8,128)(2,1)} %kv_cache.1, s32[16]{0:T(128)} %lengths.1, f32[1,256]{1,0:T(1,128)} %bitcast.7, ...), custom_call_target="tpu_custom_call" | custom-call | tf_op jit(solution)/shard_map/pallas_call | solution.py:483
  42.7 1.3 %copy.20 = bf16[16,512]{1,0:T(8,128)(2,1)} copy(bf16[16,512]{1,0:T(8,128)(2,1)} %shard_map.172) | data formatting | bytes 32768
